TPU v7x, 512 devices: a whole 4x4x16 slice. The times are simulated.
512 devices in a mesh: sp: 32 (over z, core), tp: 16 (over y, x).
Axes of the slice: x: 4, y: 4, z: 16, core: 2. Of those that a mesh axis runs over, the one named last changes fastest.
Arguments:
- residual_in: bfloat16 [8192, 2048], P('sp'), may hold values from -3 to 3
- mix_gain: float32 [2048], replicated, may hold values from 0.1 to 1.9
- pool_weight: bfloat16 [512, 2048], P(None, 'tp'), may hold values from -0.5 to 0.5
- pool_scale: float32 [2048], P('tp'), may hold values from 0.1 to 1.9
- ffn_gain: float32 [2048], replicated, may hold values from 0.1 to 1.9
- route_ids: int32 [8192, 2], P('sp'), may hold values from 0 to 31, all different within a row; in each aligned block of 16 rows (0 to 15, 16 to 31, ...) at most 2 rows name the same one
- route_weights: float32 [8192, 2], P('sp'), may hold values from 0.1 to 1
- gate_weight: bfloat16 [32, 2048, 3584], P('sp', None, 'tp'), may hold values from -0.125 to 0.125
- up_weight: bfloat16 [32, 2048, 3584], P('sp', None, 'tp'), may hold values from -0.125 to 0.125
- down_weight: bfloat16 [32, 3584, 2048], P('sp', 'tp'), may hold values from -0.09375 to 0.09375
Outputs:
- layer_out: bfloat16 [8192, 2048], P('sp')
Inputs may be any that keep to these rules, and one draw needn't show every extreme that they name: `route_ids`: each row names 2 different experts; in each aligned block of 16 rows no expert is named by more than 2 rows, and some block has an expert named by exactly 2 rows.
All inputs are finite; a program needn't handle non-finite values.
Results may differ from a plain program's by a relative error of at most 0.0074.
Values may be sent and summed in bfloat16 or wider, within the bound.
No kernel may reach another device: no remote copies, remote signals or barrier semaphores. Data moves between devices by JAX's collectives and lax.ppermute only.
A program may use at most 64 MiB of HBM per device.

v0:
```python
import jax
import jax.numpy as jnp
from jax import lax
from jax.sharding import Mesh
from jax.sharding import PartitionSpec as P

GROUPS = 4
SPAN = 16
TOP_K = 2
SP = ("sp_0", "sp_1")
EPS = 1e-06


def from_behind(value, axis, steps):
    count = lax.axis_size(axis)
    first, last = (max(0, -steps), min(count, count - steps))
    return lax.ppermute(value, axis, [(source, source + steps) for source in range(first, last)])


def split_up(shard, dim, size):
    before, after = (shard.shape[:dim], shard.shape[dim + 1 :])
    return jnp.moveaxis(shard.reshape(*before, size, -1, *after), dim, 0)


def sent_and_summed(shard, axis, dim):
    size = lax.axis_size(axis)
    blocks = lax.all_to_all(split_up(shard, dim, size), axis, 0, 0, tiled=True)
    return jnp.sum(blocks.astype(jnp.float32), axis=0)


def in_order(blocks, dim):
    dims = list(blocks.shape[1:])
    dims[dim] *= blocks.shape[0]
    return jnp.moveaxis(blocks, 0, dim).reshape(dims)


def exchange_in_order(blocks, axes, order):
    dims = [lax.axis_size(a) for a in axes]
    blocks = blocks.reshape(*dims, *blocks.shape[1:])
    for k in order:
        blocks = lax.all_to_all(blocks, axes[k], split_axis=k, concat_axis=k, tiled=True)
    return blocks.reshape(-1, *blocks.shape[len(axes) :])


def core_and_chips(shard, groups, order, split_dim, concat_dim):
    size = lax.axis_size(groups[0]) * lax.axis_size(groups[1])
    blocks = split_up(shard, split_dim, size)
    return in_order(exchange_in_order(blocks, groups, order), concat_dim)


def copy_for_each(shard, axis):
    size = lax.axis_size(axis)
    return lax.all_to_all(
        jnp.broadcast_to(shard[None], (size, *shard.shape)), axis, 0, 0, tiled=True
    )


def gather_directly(shard, axis, dim):
    blocks = copy_for_each(shard, axis)
    return in_order(blocks, dim)


def rms_scale(values, gain):
    return values * lax.rsqrt(jnp.mean(values * values, axis=-1, keepdims=True) + EPS) * gain


def slot_table(chosen_ids, experts, capacity):
    flat_ids = chosen_ids.reshape(-1)
    matches = (flat_ids[:, None] == jnp.arange(experts, dtype=jnp.int32)[None, :]).astype(jnp.int32)
    before = jnp.cumsum(matches, axis=0) - matches
    slot_of = jnp.sum(before * matches, axis=1)
    target = flat_ids * capacity + slot_of
    return (target[:, None] == jnp.arange(experts * capacity, dtype=jnp.int32)[None, :]).astype(
        jnp.float32
    )


def shards(
    residual_in,
    mix_gain,
    pool_weight,
    pool_scale,
    ffn_gain,
    route_ids,
    route_weights,
    gate_weight,
    up_weight,
    down_weight,
):
    tp_count = lax.axis_size("tp")
    sp_count = lax.axis_size(SP)
    tp_index = lax.axis_index("tp")
    tok_count, width = residual_in.shape
    group_width = width // GROUPS
    col_count = pool_weight.shape[1]
    row_count = tok_count // tp_count
    capacity = 2 * TOP_K * row_count // sp_count
    group_index = tp_index * col_count // group_width
    window = jnp.power(2, group_index + 1)
    stream = residual_in.astype(jnp.float32)
    inverse = lax.rsqrt(jnp.mean(stream * stream, axis=-1, keepdims=True) + EPS)
    stream_group = lax.dynamic_slice_in_dim(stream, group_index * group_width, group_width, 1)
    gain_group = lax.dynamic_slice_in_dim(mix_gain, group_index * group_width, group_width, 0)
    normed_group = (stream_group * inverse * gain_group).astype(jnp.bfloat16)
    rim_rows = from_behind(normed_group[tok_count - SPAN :], SP, 1)
    extended = jnp.concatenate([rim_rows, normed_group], axis=0).astype(jnp.float32)
    window_sum = jnp.zeros((tok_count, group_width), jnp.float32)
    for offset in range(SPAN):
        window_sum = window_sum + jnp.where(
            offset < window, extended[SPAN - offset : SPAN - offset + tok_count], 0.0
        )
    position = lax.axis_index(SP) * tok_count + jnp.arange(tok_count, dtype=jnp.int32)
    divisor = jnp.minimum(position + 1, window).astype(jnp.float32)
    pooled = (window_sum / divisor[:, None] - extended[SPAN:]).astype(jnp.bfloat16)
    mixed = (jnp.dot(pooled, pool_weight, preferred_element_type=jnp.float32) * pool_scale).astype(
        jnp.bfloat16
    )
    stream_own = lax.dynamic_slice_in_dim(stream, tp_index * row_count, row_count, 0)
    mixed_own = lax.all_to_all(mixed, "tp", split_axis=0, concat_axis=1, tiled=True)
    after_own = (stream_own + mixed_own.astype(jnp.float32)).astype(jnp.bfloat16)
    normed_own = rms_scale(after_own.astype(jnp.float32), ffn_gain).astype(jnp.bfloat16)
    ids_own = lax.dynamic_slice_in_dim(route_ids, tp_index * row_count, row_count, 0)
    table_own = slot_table(ids_own, sp_count, capacity)
    repeated = jnp.repeat(normed_own, TOP_K, axis=0)
    outgoing = lax.dot_general(
        table_own.astype(jnp.bfloat16),
        repeated,
        (((0,), (0,)), ((), ())),
        preferred_element_type=jnp.float32,
    )
    outgoing = outgoing.astype(jnp.bfloat16).reshape(sp_count, capacity, width)
    arrived = lax.all_to_all(outgoing, SP, split_axis=0, concat_axis=0, tiled=True)
    piece = lax.all_gather(arrived, "tp", axis=0, tiled=True)
    flat_rows = piece.reshape(-1, width)
    gate_part = jnp.dot(flat_rows, gate_weight[0], preferred_element_type=jnp.float32)
    up_part = jnp.dot(flat_rows, up_weight[0], preferred_element_type=jnp.float32)
    hidden = (jax.nn.silu(gate_part) * up_part).astype(jnp.bfloat16)
    hidden_all = hidden.reshape(piece.shape[0], piece.shape[1], hidden.shape[1])
    hidden_flat = hidden_all.reshape(-1, hidden_all.shape[-1])
    term = jnp.dot(hidden_flat, down_weight[0], preferred_element_type=jnp.float32)
    summed = sent_and_summed(
        term.astype(jnp.bfloat16).astype(jnp.float32).astype(jnp.bfloat16), "tp", 0
    )
    expert_out = summed.astype(jnp.bfloat16).reshape(sp_count, capacity, width)
    returned_rows = core_and_chips(expert_out, ("sp_0", "sp_1"), (1, 0), 0, 0)
    weights_own = lax.dynamic_slice_in_dim(route_weights, tp_index * row_count, row_count, 0)
    weight_table = jnp.einsum(
        "rk,rkc->rc", weights_own, table_own.reshape(row_count, TOP_K, sp_count * capacity)
    )
    expert_mix = jnp.dot(
        weight_table,
        returned_rows.reshape(-1, width).astype(jnp.float32),
        precision=lax.Precision.HIGHEST,
    )
    out_own = (after_own.astype(jnp.float32) + expert_mix).astype(jnp.bfloat16)
    return gather_directly(out_own, "tp", 0)


def solution(mesh):
    torus = Mesh(mesh.devices.reshape(16, 2, mesh.shape["tp"]), ("sp_0", "sp_1", "tp"))
    return jax.shard_map(
        shards,
        mesh=torus,
        in_specs=(
            P(SP, None),
            P(),
            P(None, "tp"),
            P("tp"),
            P(),
            P(SP, None),
            P(SP, None),
            P(SP, None, "tp"),
            P(SP, None, "tp"),
            P(SP, "tp", None),
        ),
        out_specs=P(SP, None),
        check_vma=False,
    )
```

profile of v0, /device:TPU:32, one launch (start us, length us, event | category | flops | bytes accessed | tf_op | source)
XLA Modules:
  0.0 268.7 jit_solution(1426922073096499499)
XLA Ops:
  6.5 1.6 multiply_reduce_fusion
  8.1 1.5 convert_element_type.67
  9.6 0.8 dynamic_slice.17
  10.4 0.1 multiply_convert_fusion
  10.5 1.9 collective-permute-start
  12.9 0.2 select_reduce_fusion
  13.1 2.5 collective-permute-done
  15.7 2.0 fusion.2
  17.7 7.0 %all-to-all-start = ((bf16[16,16,128]{2,1,0:T(8,128)(2,1)}), bf16[16,16,128]{2,1,0:T(8,128)(2,1)S(1)}, u32[]{:S(2)}, u32[]{:S(2)}) async-start(bf16[16,16,128]{2,1,0:T(8,128)(2,1)} %bitcast), calls=%async_computation | async-start | bytes 131072 | tf_op jit(solution)/shard_map/all_to_all | solution.py:119
  24.8 7.6 %all-to-all-done = bf16[16,16,128]{2,1,0:T(8,128)(2,1)S(1)} async-done(((bf16[16,16,128]{2,1,0:T(8,128)(2,1)}), bf16[16,16,128]{2,1,0:T(8,128)(2,1)S(1)}, u32[]{:S(2)}, u32[]{:S(2)}) %all-to-all-start) | async-done | bytes 65568 | tf_op jit(solution)/shard_map/all_to_all | solution.py:119
  32.4 0.1 fusion.33
  32.8 0.3 convolution_convert_fusion.1
  33.2 0.2 reshape.68
  33.3 37.4 %all_to_all.38 = bf16[32,2,2048]{2,1,0:T(2,128)(2,1)} all-to-all(bf16[32,2,2048]{2,1,0:T(2,128)(2,1)S(1)} %reshape.68), channel_id=1, replica_groups=mesh['sp_0'=16,'sp_1'=2,'tp'=16] {'sp_0','sp_1'}, dimensions={0} | all-to-all | bytes 524288 | tf_op jit(solution)/shard_map/all_to_all | solution.py:132
  70.8 56.0 %all-gather.2.cloned.1.call-done = bf16[512,2,2048]{2,1,0:T(2,128)(2,1)} async-done(((bf16[32,2,2048]{2,1,0:T(2,128)(2,1)}), bf16[512,2,2048]{2,1,0:T(2,128)(2,1)}) %all-gather.2.cloned.1.call-update) | async-done | bytes 4194320 | tf_op jit(solution)/shard_map/all_gather | solution.py:133
  126.8 7.2 %reshape.69 = bf16[1024,2048]{1,0:T(8,128)(2,1)} reshape(bf16[512,2,2048]{2,1,0:T(2,128)(2,1)} %all-gather.2.cloned.1.call-done) | data formatting | bytes 8388608 | tf_op jit(solution)/shard_map/reshape | solution.py:134
  134.0 4.6 %fusion.6 = f32[1024,224]{0,1:T(8,128)} fusion(bf16[1024,2048]{1,0:T(8,128)(2,1)} %reshape.69, bf16[1,2048,224]{1,2,0:T(8,128)(2,1)S(1)} %copy-done.3), kind=kOutput, calls=%fused_computation.11 | convolution fusion | flops 939524096 | bytes 6029312 | tf_op jit(solution)/shard_map/dot_general | solution.py:135
  138.6 7.0 %convolution_convert_fusion = bf16[1024,2048]{1,0:T(8,128)(2,1)} fusion(bf16[1024,2048]{1,0:T(8,128)(2,1)} %reshape.69, bf16[1,224,2048]{2,1,0:T(8,128)(2,1)S(1)} %copy-done, bf16[1,2048,224]{1,2,0:T(8,128)(2,1)S(1)} %copy-done.4, f32[1024,224]{0,1:T(8,128)} %fusion.6), kind=kOutput, calls=%fused_computation | convolution fusion | flops 1882521600 | bytes 11141120 | tf_op jit(solution)/shard_map/dot_general | solution.py:140
  145.6 56.0 %all_to_all.39 = bf16[16,64,2048]{2,1,0:T(8,128)(2,1)} all-to-all(bf16[16,64,2048]{2,1,0:T(8,128)(2,1)} %bitcast.35), channel_id=1, replica_groups=mesh['sp_0'=16,'sp_1'=2,'tp'=16] {'tp'}, dimensions={0} | all-to-all | bytes 8388608 | tf_op jit(solution)/shard_map/all_to_all | solution.py:27
  201.7 3.0 %reduce_sum.45 = bf16[64,2048]{1,0:T(8,128)(2,1)S(1)} reduce(bf16[16,64,2048]{2,1,0:T(8,128)(2,1)} %all_to_all.39, bf16[]{:T(256)} %constant.97.clone.1), dimensions={0}, to_apply=%region_4.5 | reduce | flops 1966080 | bytes 4456450 | tf_op jit(solution)/shard_map/reduce_sum | solution.py:28
  204.6 0.2 reshape_reshape_reshape.6
  204.8 0.2 copy.20
  205.0 3.9 %all_to_all.40 = bf16[16,2,1,2,2048]{4,3,0,2,1:T(2,128)(2,1)S(1)} all-to-all(bf16[16,2,1,2,2048]{4,3,0,2,1:T(2,128)(2,1)S(1)} %copy.20), channel_id=1, replica_groups=mesh['sp_0'=16,'sp_1'=2,'tp'=16] {'sp_1'}, dimensions={1} | all-to-all | bytes 524288 | tf_op jit(solution)/shard_map/all_to_all | solution.py:41
  209.0 1.0 copy.21
  209.9 12.7 %all-to-all-start.4 = ((bf16[16,2,1,2,2048]{4,3,1,2,0:T(2,128)(2,1)}), bf16[16,2,1,2,2048]{4,3,1,2,0:T(2,128)(2,1)S(1)}, u32[]{:S(2)}, u32[]{:S(2)}) async-start(bf16[16,2,1,2,2048]{4,3,1,2,0:T(2,128)(2,1)} %copy.21), calls=%async_computation.4 | async-start | bytes 524288 | tf_op jit(solution)/shard_map/all_to_all | solution.py:41
  222.7 0.8 dynamic-slice_bitcast_fusion
  223.5 0.2 fusion.37
  223.7 17.2 %all-to-all-done.4 = bf16[16,2,1,2,2048]{4,3,1,2,0:T(2,128)(2,1)S(1)} async-done(((bf16[16,2,1,2,2048]{4,3,1,2,0:T(2,128)(2,1)}), bf16[16,2,1,2,2048]{4,3,1,2,0:T(2,128)(2,1)S(1)}, u32[]{:S(2)}, u32[]{:S(2)}) %all-to-all-start.4) | async-done | bytes 262176 | tf_op jit(solution)/shard_map/all_to_all | solution.py:41
  241.1 0.2 fusion
  241.3 0.1 broadcast_in_dim.39
  241.4 19.5 %all_to_all.41 = bf16[16,16,2048]{2,1,0:T(8,128)(2,1)S(1)} all-to-all(bf16[16,16,2048]{2,1,0:T(8,128)(2,1)S(1)} %broadcast_in_dim.39), channel_id=1, replica_groups=mesh['sp_0'=16,'sp_1'=2,'tp'=16] {'tp'}, dimensions={0} | all-to-all | bytes 2097152 | tf_op jit(solution)/shard_map/all_to_all | solution.py:53
  260.9 1.0 copy.29
  (34 shorter events, 1.0 us)
Async XLA Ops:
  6.5 132.1 %copy-start = (bf16[1,224,2048]{2,1,0:T(8,128)(2,1)S(1)}, bf16[1,224,2048]{2,1,0:T(8,128)(2,1)}, u32[]{:S(2)}) copy-start(bf16[1,224,2048]{2,1,0:T(8,128)(2,1)} %param.19) | copy-start | bytes 2752516
  6.5 6.0 %copy-start.2 = (s32[256,2]{0,1:T(2,128)S(1)}, s32[256,2]{0,1:T(2,128)}, u32[]{:S(2)}) copy-start(s32[256,2]{0,1:T(2,128)} %param.15) | copy-start | bytes 6148
  6.5 9.1 %copy-start.6 = (f32[128]{0:T(128)S(1)}, f32[128]{0:T(128)}, u32[]{:S(2)}) copy-start(f32[128]{0:T(128)} %param.13) | copy-start | bytes 1540
  6.5 9.1 %copy-start.5 = (bf16[512,128]{1,0:T(8,128)(2,1)S(1)}, bf16[512,128]{1,0:T(8,128)(2,1)}, u32[]{:S(2)}) copy-start(bf16[512,128]{1,0:T(8,128)(2,1)} %param.12) | copy-start | bytes 393220
  10.5 5.1 %collective-permute-start = (bf16[16,512]{1,0:T(8,128)(2,1)S(1)}, bf16[16,512]{1,0:T(8,128)(2,1)S(1)}, u32[]{:S(2)}, u32[]{:S(2)}) collective-permute-start(bf16[16,512]{1,0:T(8,128)(2,1)S(1)} %slice.69), channel_id=1, source_target_pairs={{0,16},{16,32},{32,48},{48,64},{64,80},{80,96},{96,112},{112,128},... | collective-permute-start | bytes 49160 | tf_op jit(solution)/shard_map/ppermute | solution.py:17
  15.7 16.9 %copy-start.1 = (f32[2048]{0:T(1024)S(1)}, f32[2048]{0:T(1024)}, u32[]{:S(2)}) copy-start(f32[2048]{0:T(1024)} %param.14) | copy-start | bytes 24580
  17.7 14.7 %all-to-all-start = ((bf16[16,16,128]{2,1,0:T(8,128)(2,1)}), bf16[16,16,128]{2,1,0:T(8,128)(2,1)S(1)}, u32[]{:S(2)}, u32[]{:S(2)}) async-start(bf16[16,16,128]{2,1,0:T(8,128)(2,1)} %bitcast), calls=%async_computation | async-start | bytes 131072 | tf_op jit(solution)/shard_map/all_to_all | solution.py:119
  24.8 102.0 %all-gather.2.cloned.1.call-start = ((), (), s32[]{:S(2)}) async-start(), calls=%async_computation.6 | async-start | bytes 4456448 | tf_op jit(solution)/shard_map/all_gather | solution.py:133
  70.8 63.2 %copy-start.3 = (bf16[1,2048,224]{1,2,0:T(8,128)(2,1)S(1)}, bf16[1,2048,224]{1,2,0:T(8,128)(2,1)}, u32[]{:S(2)}) copy-start(bf16[1,2048,224]{1,2,0:T(8,128)(2,1)} %param.17) | copy-start | bytes 2752516
  134.0 4.6 %copy-start.4 = (bf16[1,2048,224]{1,2,0:T(8,128)(2,1)S(1)}, bf16[1,2048,224]{1,2,0:T(8,128)(2,1)}, u32[]{:S(2)}) copy-start(bf16[1,2048,224]{1,2,0:T(8,128)(2,1)} %param.18) | copy-start | bytes 2752516
  209.9 31.0 %all-to-all-start.4 = ((bf16[16,2,1,2,2048]{4,3,1,2,0:T(2,128)(2,1)}), bf16[16,2,1,2,2048]{4,3,1,2,0:T(2,128)(2,1)S(1)}, u32[]{:S(2)}, u32[]{:S(2)}) async-start(bf16[16,2,1,2,2048]{4,3,1,2,0:T(2,128)(2,1)} %copy.21), calls=%async_computation.4 | async-start | bytes 524288 | tf_op jit(solution)/shard_map/all_to_all | solution.py:41
Sparse Core Ops, SparseCore 0:
  70.9 55.8 all-gather.1
where the time goes:
time: 269 us
  blocking collectives  117 us (43%)
  waiting for transfers between devices  83.3 us (31%)
  starting transfers between devices  21.7 us (8%)
  matrix products  14.4 us (5%)
  between operations  13.7 us (5%)
  local copies, waits for them, and re-layouts  12 us (4%)
  other arithmetic  6.75 us (3%)
    all_to_all x1, blocking collectives, sent_and_summed(): blocks = lax.all_to_all(split_up(shard, dim, size), axis, 0, 0, tiled=True)  56 us
    all_gather x1, waiting for transfers between devices, shards(): piece = lax.all_gather(arrived, 'tp', axis=0, tiled=True)  56 us
    all_to_all x1, blocking collectives, shards(): lax.all_to_all(outgoing, SP, split_axis=0, concat_axis=0, tiled=True)  37.4 us
    all_to_all x1, blocking collectives, copy_for_each(): lax.all_to_all(jnp.broadcast_to(shard[None], (size, *shard.shape)), axis,...  19.5 us
    all_to_all x1, waiting for transfers between devices, exchange_in_order(): lax.all_to_all(blocks, axes[k], split_axis=k, concat_axis=k, tiled=True)  17.2 us
    all_to_all x1, starting transfers between devices, exchange_in_order(): lax.all_to_all(blocks, axes[k], split_axis=k, concat_axis=k, tiled=True)  12.7 us
    all_to_all x1, waiting for transfers between devices, shards(): lax.all_to_all(mixed, 'tp', split_axis=0, concat_axis=1, tiled=True)  7.6 us
    reshape x1, local copies, waits for them, and re-layouts, shards(): flat_rows = piece.reshape(-1, width)  7.21 us
  transfers between devices with their start and end apart: 4, of which 4 were waited for; matrix products, arithmetic and copies ran while one was open for 1% of the time, Pallas kernels for 0%

commit v1 on v0

--- a/solution.py
+++ b/solution.py
@@ -9,6 +9,11 @@
 TOP_K = 2
 SP = ("sp_0", "sp_1")
 EPS = 1e-06
+
+
+def tiled_gather(x, axis, dim):
+    copies = jnp.concatenate([x] * lax.axis_size(axis), axis=dim)
+    return lax.all_to_all(copies, axis, dim, dim, tiled=True)
 
 
 def from_behind(value, axis, steps):
@@ -130,7 +135,7 @@
     )
     outgoing = outgoing.astype(jnp.bfloat16).reshape(sp_count, capacity, width)
     arrived = lax.all_to_all(outgoing, SP, split_axis=0, concat_axis=0, tiled=True)
-    piece = lax.all_gather(arrived, "tp", axis=0, tiled=True)
+    piece = tiled_gather(arrived, "tp", 0)
     flat_rows = piece.reshape(-1, width)
     gate_part = jnp.dot(flat_rows, gate_weight[0], preferred_element_type=jnp.float32)
     up_part = jnp.dot(flat_rows, up_weight[0], preferred_element_type=jnp.float32)

time: 269 us -> 251 us (0.933)
  waiting for transfers between devices: 83.3 us -> 27.3 us
  blocking collectives: 117 us -> 170 us
  between operations: 13.7 us -> 0.34 us
  starting transfers between devices: 21.7 us -> 15.7 us
  local copies, waits for them, and re-layouts: 12 us -> 15.4 us
    all_gather x1 -> x0, waiting for transfers between devices: 56 us -> none  [shards(): piece = lax.all_gather(arrived, 'tp', axis=0, tiled=True)]
    all_to_all x0 -> x1, blocking collectives: none -> 53.8 us  [tiled_gather(): return lax.all_to_all(copies, axis, dim, dim, tiled=True)]
    all_to_all x1, starting transfers between devices: 12.7 us -> 6.77 us  [exchange_in_order(): lax.all_to_all(blocks, axes[k], split_axis=k, concat_axis=k, tiled=True)]
    unnamed x16 -> x31, local copies, waits for them, and re-layouts: 1.09 us -> 4.17 us
  transfers between devices with their start and end apart: 4 -> 3, of which waited for: 4 -> 3; matrix products, arithmetic and copies ran while one was open for 1% -> 1% of each run, Pallas kernels for 0% -> 0%
where the time goes in v1:
time: 251 us; the launch traced here: 250 us
  blocking collectives  170 us (68%)
  waiting for transfers between devices  27.3 us (11%)
  starting transfers between devices  15.7 us (6%)
  local copies, waits for them, and re-layouts  15.4 us (6%)
  matrix products  14.4 us (6%)
  other arithmetic  6.75 us (3%)
    all_to_all x1, blocking collectives, sent_and_summed(): blocks = lax.all_to_all(split_up(shard, dim, size), axis, 0, 0, tiled=True)  55.4 us
    all_to_all x1, blocking collectives, tiled_gather(): return lax.all_to_all(copies, axis, dim, dim, tiled=True)  53.8 us
    all_to_all x1, blocking collectives, shards(): lax.all_to_all(outgoing, SP, split_axis=0, concat_axis=0, tiled=True)  37.3 us
    all_to_all x1, blocking collectives, copy_for_each(): lax.all_to_all(jnp.broadcast_to(shard[None], (size, *shard.shape)), axis,...  19.4 us
    all_to_all x1, waiting for transfers between devices, exchange_in_order(): lax.all_to_all(blocks, axes[k], split_axis=k, concat_axis=k, tiled=True)  17.2 us
    all_to_all x1, waiting for transfers between devices, shards(): lax.all_to_all(mixed, 'tp', split_axis=0, concat_axis=1, tiled=True)  7.65 us
    reshape x1, local copies, waits for them, and re-layouts, shards(): flat_rows = piece.reshape(-1, width)  7.29 us
    all_to_all x1, starting transfers between devices, shards(): lax.all_to_all(mixed, 'tp', split_axis=0, concat_axis=1, tiled=True)  7.03 us
  transfers between devices with their start and end apart: 3, of which 3 were waited for; matrix products, arithmetic and copies ran while one was open for 1% of the time, Pallas kernels for 0%

profile of v1, /device:TPU:32, one launch (start us, length us, event | category | flops | bytes accessed | tf_op | source)
XLA Modules:
  0.0 249.9 jit_solution(2664294725532684490)
XLA Ops:
  0.0 1.6 multiply_reduce_fusion
  1.6 1.5 convert_element_type.67
  3.1 0.8 dynamic_slice.17
  4.0 1.9 collective-permute-start
  6.6 2.5 collective-permute-done
  9.2 2.0 fusion.2
  11.2 7.0 %all-to-all-start = ((bf16[16,16,128]{2,1,0:T(8,128)(2,1)}), bf16[16,16,128]{2,1,0:T(8,128)(2,1)S(1)}, u32[]{:S(2)}, u32[]{:S(2)}) async-start(bf16[16,16,128]{2,1,0:T(8,128)(2,1)} %bitcast), calls=%async_computation | async-start | bytes 131072 | tf_op jit(solution)/shard_map/all_to_all | solution.py:124
  18.3 7.7 %all-to-all-done = bf16[16,16,128]{2,1,0:T(8,128)(2,1)S(1)} async-done(((bf16[16,16,128]{2,1,0:T(8,128)(2,1)}), bf16[16,16,128]{2,1,0:T(8,128)(2,1)S(1)}, u32[]{:S(2)}, u32[]{:S(2)}) %all-to-all-start) | async-done | bytes 65568 | tf_op jit(solution)/shard_map/all_to_all | solution.py:124
  26.3 0.3 convolution_convert_fusion.1
  26.8 37.3 %all_to_all.43 = bf16[32,2,2048]{2,1,0:T(2,128)(2,1)S(1)} all-to-all(bf16[32,2,2048]{2,1,0:T(2,128)(2,1)S(1)} %reshape.68), channel_id=1, replica_groups=mesh['sp_0'=16,'sp_1'=2,'tp'=16] {'sp_0','sp_1'}, dimensions={0} | all-to-all | bytes 524288 | tf_op jit(solution)/shard_map/all_to_all | solution.py:137
  64.3 0.2 constant_dynamic-update-slice_fusion.14
  64.5 0.2 constant_dynamic-update-slice_fusion.13
  64.8 0.2 constant_dynamic-update-slice_fusion.12
  65.4 0.2 constant_dynamic-update-slice_fusion.9
  65.6 0.2 constant_dynamic-update-slice_fusion.8
  66.2 0.2 constant_dynamic-update-slice_fusion.5
  67.0 0.2 constant_dynamic-update-slice_fusion.1
  67.5 53.8 %all_to_all.44 = bf16[512,2,2048]{2,1,0:T(2,128)(2,1)} all-to-all(bf16[512,2,2048]{2,1,0:T(2,128)(2,1)S(1)} %constant_dynamic-update-slice_fusion), channel_id=1, replica_groups=mesh['sp_0'=16,'sp_1'=2,'tp'=16] {'tp'}, dimensions={0} | all-to-all | bytes 8388608 | tf_op jit(solution)/shard_map/all_to_all | solution.py:16
  121.3 7.3 %reshape.69 = bf16[1024,2048]{1,0:T(8,128)(2,1)} reshape(bf16[512,2,2048]{2,1,0:T(2,128)(2,1)} %all_to_all.44) | data formatting | bytes 8388608 | tf_op jit(solution)/shard_map/reshape | solution.py:139
  128.6 4.6 %fusion.6 = f32[1024,224]{0,1:T(8,128)} fusion(bf16[1024,2048]{1,0:T(8,128)(2,1)} %reshape.69, bf16[1,2048,224]{1,2,0:T(8,128)(2,1)S(1)} %copy-done.3), kind=kOutput, calls=%fused_computation.11 | convolution fusion | flops 939524096 | bytes 6029312 | tf_op jit(solution)/shard_map/dot_general | solution.py:140
  133.2 7.0 %convolution_convert_fusion = bf16[1024,2048]{1,0:T(8,128)(2,1)} fusion(bf16[1024,2048]{1,0:T(8,128)(2,1)} %reshape.69, bf16[1,224,2048]{2,1,0:T(8,128)(2,1)S(1)} %copy-done, bf16[1,2048,224]{1,2,0:T(8,128)(2,1)S(1)} %copy-done.4, f32[1024,224]{0,1:T(8,128)} %fusion.6), kind=kOutput, calls=%fused_computation | convolution fusion | flops 1882521600 | bytes 11141120 | tf_op jit(solution)/shard_map/dot_general | solution.py:145
  140.2 55.4 %all_to_all.45 = bf16[16,64,2048]{2,1,0:T(8,128)(2,1)} all-to-all(bf16[16,64,2048]{2,1,0:T(8,128)(2,1)} %bitcast.35), channel_id=1, replica_groups=mesh['sp_0'=16,'sp_1'=2,'tp'=16] {'tp'}, dimensions={0} | all-to-all | bytes 8388608 | tf_op jit(solution)/shard_map/all_to_all | solution.py:32
  195.6 3.0 %reduce_sum.45 = bf16[64,2048]{1,0:T(8,128)(2,1)S(1)} reduce(bf16[16,64,2048]{2,1,0:T(8,128)(2,1)} %all_to_all.45, bf16[]{:T(256)} %constant.97.clone.1), dimensions={0}, to_apply=%region_4.5 | reduce | flops 1966080 | bytes 4456450 | tf_op jit(solution)/shard_map/reduce_sum | solution.py:33
  199.0 3.9 %all_to_all.46 = bf16[16,2,1,2,2048]{4,3,0,2,1:T(2,128)(2,1)S(1)} all-to-all(bf16[16,2,1,2,2048]{4,3,0,2,1:T(2,128)(2,1)S(1)} %copy.20), channel_id=1, replica_groups=mesh['sp_0'=16,'sp_1'=2,'tp'=16] {'sp_1'}, dimensions={1} | all-to-all | bytes 524288 | tf_op jit(solution)/shard_map/all_to_all | solution.py:46
  202.9 1.0 copy.21
  203.9 6.8 %all-to-all-start.5 = ((bf16[16,2,1,2,2048]{4,3,1,2,0:T(2,128)(2,1)}), bf16[16,2,1,2,2048]{4,3,1,2,0:T(2,128)(2,1)S(1)}, u32[]{:S(2)}, u32[]{:S(2)}) async-start(bf16[16,2,1,2,2048]{4,3,1,2,0:T(2,128)(2,1)} %copy.21), calls=%async_computation.5 | async-start | bytes 524288 | tf_op jit(solution)/shard_map/all_to_all | solution.py:46
  210.7 0.8 dynamic-slice_bitcast_fusion
  211.6 0.2 fusion.37
  211.8 17.2 %all-to-all-done.5 = bf16[16,2,1,2,2048]{4,3,1,2,0:T(2,128)(2,1)S(1)} async-done(((bf16[16,2,1,2,2048]{4,3,1,2,0:T(2,128)(2,1)}), bf16[16,2,1,2,2048]{4,3,1,2,0:T(2,128)(2,1)S(1)}, u32[]{:S(2)}, u32[]{:S(2)}) %all-to-all-start.5) | async-done | bytes 262176 | tf_op jit(solution)/shard_map/all_to_all | solution.py:46
  229.1 0.2 fusion
  229.5 19.4 %all_to_all.47 = bf16[16,16,2048]{2,1,0:T(8,128)(2,1)S(1)} all-to-all(bf16[16,16,2048]{2,1,0:T(8,128)(2,1)S(1)} %broadcast_in_dim.39), channel_id=1, replica_groups=mesh['sp_0'=16,'sp_1'=2,'tp'=16] {'tp'}, dimensions={0} | all-to-all | bytes 2097152 | tf_op jit(solution)/shard_map/all_to_all | solution.py:58
  248.9 1.0 copy.44
  (48 shorter events, 3.9 us)
Async XLA Ops:
  0.0 133.2 %copy-start = (bf16[1,224,2048]{2,1,0:T(8,128)(2,1)S(1)}, bf16[1,224,2048]{2,1,0:T(8,128)(2,1)}, u32[]{:S(2)}) copy-start(bf16[1,224,2048]{2,1,0:T(8,128)(2,1)} %param.19) | copy-start | bytes 2752516
  0.0 6.0 %copy-start.2 = (s32[256,2]{0,1:T(2,128)S(1)}, s32[256,2]{0,1:T(2,128)}, u32[]{:S(2)}) copy-start(s32[256,2]{0,1:T(2,128)} %param.15) | copy-start | bytes 6148
  0.0 9.1 %copy-start.6 = (f32[128]{0:T(128)S(1)}, f32[128]{0:T(128)}, u32[]{:S(2)}) copy-start(f32[128]{0:T(128)} %param.13) | copy-start | bytes 1540
  0.0 9.1 %copy-start.5 = (bf16[512,128]{1,0:T(8,128)(2,1)S(1)}, bf16[512,128]{1,0:T(8,128)(2,1)}, u32[]{:S(2)}) copy-start(bf16[512,128]{1,0:T(8,128)(2,1)} %param.12) | copy-start | bytes 393220
  4.0 5.1 %collective-permute-start = (bf16[16,512]{1,0:T(8,128)(2,1)S(1)}, bf16[16,512]{1,0:T(8,128)(2,1)S(1)}, u32[]{:S(2)}, u32[]{:S(2)}) collective-permute-start(bf16[16,512]{1,0:T(8,128)(2,1)S(1)} %slice.69), channel_id=1, source_target_pairs={{0,16},{16,32},{32,48},{48,64},{64,80},{80,96},{96,112},{112,128},... | collective-permute-start | bytes 49160 | tf_op jit(solution)/shard_map/ppermute | solution.py:22
  9.2 16.9 %copy-start.1 = (f32[2048]{0:T(1024)S(1)}, f32[2048]{0:T(1024)}, u32[]{:S(2)}) copy-start(f32[2048]{0:T(1024)} %param.14) | copy-start | bytes 24580
  11.2 14.7 %all-to-all-start = ((bf16[16,16,128]{2,1,0:T(8,128)(2,1)}), bf16[16,16,128]{2,1,0:T(8,128)(2,1)S(1)}, u32[]{:S(2)}, u32[]{:S(2)}) async-start(bf16[16,16,128]{2,1,0:T(8,128)(2,1)} %bitcast), calls=%async_computation | async-start | bytes 131072 | tf_op jit(solution)/shard_map/all_to_all | solution.py:124
  121.3 7.3 %copy-start.3 = (bf16[1,2048,224]{1,2,0:T(8,128)(2,1)S(1)}, bf16[1,2048,224]{1,2,0:T(8,128)(2,1)}, u32[]{:S(2)}) copy-start(bf16[1,2048,224]{1,2,0:T(8,128)(2,1)} %param.17) | copy-start | bytes 2752516
  128.6 4.6 %copy-start.4 = (bf16[1,2048,224]{1,2,0:T(8,128)(2,1)S(1)}, bf16[1,2048,224]{1,2,0:T(8,128)(2,1)}, u32[]{:S(2)}) copy-start(bf16[1,2048,224]{1,2,0:T(8,128)(2,1)} %param.18) | copy-start | bytes 2752516
  203.9 25.1 %all-to-all-start.5 = ((bf16[16,2,1,2,2048]{4,3,1,2,0:T(2,128)(2,1)}), bf16[16,2,1,2,2048]{4,3,1,2,0:T(2,128)(2,1)S(1)}, u32[]{:S(2)}, u32[]{:S(2)}) async-start(bf16[16,2,1,2,2048]{4,3,1,2,0:T(2,128)(2,1)} %copy.21), calls=%async_computation.5 | async-start | bytes 524288 | tf_op jit(solution)/shard_map/all_to_all | solution.py:46
